TPU v7x, 32 devices: a whole 2x2x4 slice. The times are simulated.
32 devices in a mesh: kv: 4 (over y, x), tp: 8 (over z, core).
Axes of the slice: x: 2, y: 2, z: 4, core: 2. Of those that a mesh axis runs over, the one named last changes fastest.
Arguments:
- tokens: bfloat16 [256, 4096], P('tp', 'kv'), may hold values from -19 to 19, as said below
- lengths: int32 [256], P('kv'), may hold values from 1 to 16384, 1048576 in all
- state_block: float32 [256, 64, 2048], P('kv', None, 'tp'), may hold values from -6 to 6
- cached_keys: bfloat16 [256, 128, 2048], P('kv', None, 'tp'), may hold values from -0.75 to 0.75
- cached_values: bfloat16 [256, 128, 2048], P('kv', None, 'tp'), may hold values from -6 to 6
- query_weight: bfloat16 [4096, 2048], P('kv', 'tp'), may hold values from -0.09375 to 0.09375
- key_weight: bfloat16 [4096, 2048], P('kv', 'tp'), may hold values from -0.09375 to 0.09375
- value_weight: bfloat16 [4096, 2048], P('kv', 'tp'), may hold values from -0.09375 to 0.09375
- gate_weight: bfloat16 [4096, 2048], P('kv', 'tp'), may hold values from -0.09375 to 0.09375
- decay_rate: float32 [32], P('tp'), may hold values from 0.0005 to 0.05
- head_gain: float32 [2048], P('tp'), may hold values from 0.1 to 1.9
- out_weight: bfloat16 [2048, 4096], P('tp', 'kv'), may hold values from -0.125 to 0.125
- mixer_gain: float32 [4096], P('kv'), may hold values from 0.1 to 1.9
- up_weight: bfloat16 [4096, 16384], P('kv', 'tp'), may hold values from -0.09375 to 0.09375
- down_weight: bfloat16 [16384, 4096], P('tp', 'kv'), may hold values from -0.046875 to 0.046875
- final_gain: float32 [4096], P('kv'), may hold values from 0.1 to 1.9
Outputs:
- next_rows: bfloat16 [256, 4096], P('tp', 'kv')
Inputs may be any that keep to these rules, and one draw needn't show every extreme that they name: `tokens`: the rows' column groups have scales that differ between groups.
All inputs are finite; a program needn't handle non-finite values. No bound on the sum of `lengths` on one device may be relied on, other than what follows from the above.
Results may differ from a plain program's by a relative error of at most 0.0095.
Values may be sent and summed in bfloat16 or wider, within the bound.
A program may use at most 128 MiB of HBM per device.

v0:
```python
import jax
import jax.numpy as jnp
from jax import lax
from jax.sharding import PartitionSpec as P

HDIM = 64
BLK = 128
ALPHA = 2.0**0.5
EPS = 1e-05


def rotate(vectors, positions):
    half = vectors.shape[-1] // 2
    inverse = 10000.0 ** (-jnp.arange(half, dtype=jnp.float32) / half)
    angle = positions.astype(jnp.float32)[:, None] * inverse[None, :]
    cosine = jnp.cos(angle)[:, None, :]
    sine = jnp.sin(angle)[:, None, :]
    former, latter = (vectors[..., :half], vectors[..., half:])
    return jnp.concatenate([former * cosine - latter * sine, latter * cosine + former * sine], -1)


def normalize(values, gain):
    width = values.shape[1] * lax.axis_size("kv")
    total, square = lax.psum((jnp.sum(values, 1), jnp.sum(values * values, 1)), "kv")
    mean = total / width
    centred = values - mean[:, None]
    spread = square / width - mean * mean
    return centred * lax.rsqrt(spread[:, None] + EPS) * gain[None, :]


def retain(query, keyed, valued, gated, lengths, state, keys, values, rate, gain):
    count = query.shape[0]
    heads = rate.shape[0]
    q_rot = rotate(query.astype(jnp.float32).reshape(count, heads, HDIM), lengths).astype(
        jnp.bfloat16
    )
    k_rot = (rotate(keyed.astype(jnp.float32).reshape(count, heads, HDIM), lengths) * 0.125).astype(
        jnp.bfloat16
    )
    v_new = valued.astype(jnp.float32).reshape(count, heads, HDIM)
    cached_k = keys.reshape(count, BLK, heads, HDIM)
    cached_v = values.reshape(count, BLK, heads, HDIM)
    scores = jnp.einsum("shn,sihn->shi", q_rot, cached_k, preferred_element_type=jnp.float32)
    offset = lengths % BLK
    slots = jnp.arange(BLK, dtype=jnp.int32)
    lag = jnp.maximum(offset[:, None] - slots[None, :], 0).astype(jnp.float32)
    live = (slots[None, :] < offset[:, None])[:, None, :]
    factor = jnp.where(live, jnp.exp(-rate[None, :, None] * lag[:, None, :]), 0.0)
    weights = (scores * factor).astype(jnp.bfloat16)
    own = jnp.einsum("shn,shn->sh", q_rot, k_rot, preferred_element_type=jnp.float32).astype(
        jnp.bfloat16
    )
    inner = jnp.einsum("shi,sihn->shn", weights, cached_v, preferred_element_type=jnp.float32)
    inner = inner + own.astype(jnp.float32)[..., None] * v_new
    carried = jnp.exp(-rate[None, :] * (offset[:, None] + 1).astype(jnp.float32))
    cross = (
        jnp.einsum(
            "shk,skhv->shv",
            q_rot.astype(jnp.float32),
            state.reshape(count, HDIM, heads, HDIM),
            precision=lax.Precision.HIGHEST,
        )
        * carried[..., None]
    )
    retained = inner + cross
    mean = jnp.mean(retained, -1, keepdims=True)
    centred = retained - mean
    spread = jnp.mean(centred * centred, -1, keepdims=True)
    normed = centred * lax.rsqrt(spread + EPS) * gain.reshape(heads, HDIM)[None]
    gate_f = jax.nn.silu(gated.astype(jnp.float32).reshape(count, heads, HDIM))
    return (gate_f * normed).reshape(count, heads * HDIM).astype(jnp.bfloat16)


def per_device(
    tokens,
    lengths,
    state_block,
    cached_keys,
    cached_values,
    query_weight,
    key_weight,
    value_weight,
    gate_weight,
    decay_rate,
    head_gain,
    out_weight,
    mixer_gain,
    up_weight,
    down_weight,
    final_gain,
):
    all_rows = lax.all_gather(tokens, "tp", axis=0, tiled=True)
    width = query_weight.shape[1]
    piece = all_rows
    summed = lax.psum_scatter(
        jnp.concatenate(
            [
                jnp.dot(piece, weight, preferred_element_type=jnp.float32)
                for weight in (query_weight, key_weight, value_weight, gate_weight)
            ],
            1,
        ),
        "kv",
        scatter_dimension=0,
        tiled=True,
    ).astype(jnp.bfloat16)
    query, keyed, valued, gated = [
        summed[:, index * width : (index + 1) * width] for index in range(4)
    ]
    mixed = retain(
        query,
        keyed,
        valued,
        gated,
        lengths,
        state_block,
        cached_keys,
        cached_values,
        decay_rate,
        head_gain,
    )
    mixed_all = lax.all_gather(mixed, "kv", axis=0, tiled=True)
    piece = mixed_all
    branch = lax.psum_scatter(
        jnp.dot(piece, out_weight, preferred_element_type=jnp.float32),
        "tp",
        scatter_dimension=0,
        tiled=True,
    )
    hidden = normalize(ALPHA * tokens.astype(jnp.float32) + branch, mixer_gain).astype(jnp.bfloat16)
    hidden_all = lax.all_gather(hidden, "tp", axis=0, tiled=True)
    upward = lax.psum(jnp.dot(hidden_all, up_weight, preferred_element_type=jnp.float32), "kv")
    active = jnp.square(jax.nn.relu(upward)).astype(jnp.bfloat16)
    piece = active
    downward = lax.psum_scatter(
        jnp.dot(piece, down_weight, preferred_element_type=jnp.float32),
        "tp",
        scatter_dimension=0,
        tiled=True,
    )
    result = normalize(ALPHA * hidden.astype(jnp.float32) + downward, final_gain)
    return result.astype(jnp.bfloat16)


def solution(mesh):
    return jax.shard_map(
        per_device,
        mesh=mesh,
        in_specs=(
            P("tp", "kv"),
            P("kv"),
            P("kv", None, "tp"),
            P("kv", None, "tp"),
            P("kv", None, "tp"),
            P("kv", "tp"),
            P("kv", "tp"),
            P("kv", "tp"),
            P("kv", "tp"),
            P("tp"),
            P("tp"),
            P("tp", "kv"),
            P("kv"),
            P("kv", "tp"),
            P("tp", "kv"),
            P("kv"),
        ),
        out_specs=P("tp", "kv"),
        check_vma=False,
    )
```

profile of v0, /device:TPU:0, one launch (start us, length us, event | category | flops | bytes accessed | tf_op | source)
XLA Modules:
  0.0 271.9 jit_solution(15027838848131162646)
XLA Ops:
  6.5 16.8 %all_gather.9 = bf16[256,1024]{1,0:T(8,128)(2,1)S(1)} all-gather(bf16[32,1024]{1,0:T(8,128)(2,1)} %param.16), channel_id=1, replica_groups=mesh['kv'=4,'tp'=8] {'tp'}, dimensions={0}, use_global_device_ids=true | all-gather | bytes 589824 | tf_op jit(solution)/shard_map/all_gather | solution.py:92
  23.4 1.4 fusion.22
  24.8 1.4 fusion.23
  26.2 1.4 fusion.24
  28.0 1.3 copy.37
  29.4 6.4 %copy.19 = bf16[64,128,256]{1,2,0:T(8,128)(2,1)} copy(bf16[64,128,256]{2,1,0:T(8,128)(2,1)} %param.19) | data formatting | bytes 8388608 | tf_op args[3]
  35.8 6.4 %copy.20 = bf16[64,128,256]{1,2,0:T(8,128)(2,1)} copy(bf16[64,128,256]{2,1,0:T(8,128)(2,1)} %param.20) | data formatting | bytes 8388608 | tf_op args[4]
  42.2 8.2 %reshape.187 = f32[64,64,4,64]{3,2,1,0:T(4,128)} reshape(f32[64,64,256]{2,1,0:T(8,128)} %param.18) | data formatting | bytes 8388608 | tf_op jit(solution)/shard_map/reshape | solution.py:60
  50.8 7.7 %reduce-scatter.10.cloned.1.call-done = f32[64,1024]{1,0:T(8,128)} async-done(((f32[256,1024]{1,0:T(8,128)}), f32[64,1024]{1,0:T(8,128)}) %reduce-scatter.10.cloned.1.call-update) | async-done | bytes 262160
  60.0 3.5 %fusion.26 = f32[64,4,1,128]{3,2,1,0:T(1,128)S(1)} fusion(bf16[64,4,64,1]{2,3,1,0:T(2,128)(2,1)S(1)} %copy.22, bf16[64,128,4,64]{1,3,2,0:T(8,128)(2,1)} %bitcast.41), kind=kOutput, calls=%fused_computation.63 | convolution fusion | flops 4194304 | bytes 4358144 | tf_op jit(solution)/shard_map/shn,sihn->shi/dot_general | solution.py:43
  63.7 2.3 fusion.9
  66.1 1.9 copy.39
  68.0 6.4 %multiply_reduce_fusion = f32[64,4,64]{2,1,0:T(4,128)S(1)} fusion(f32[64,64,4,64]{3,2,1,0:T(4,128)} %reshape.187, f32[64,4,64]{1,2,0:T(8,128)S(1)} %copy.39), kind=kLoop, calls=%fused_computation | loop fusion | flops 2080768 | bytes 4325376
  74.8 8.5 %all_gather.10 = bf16[256,256]{1,0:T(8,128)(2,1)S(1)} all-gather(bf16[64,256]{1,0:T(8,128)(2,1)S(1)} %copy.36), channel_id=1, replica_groups=mesh['kv'=4,'tp'=8] {'kv'}, dimensions={0}, use_global_device_ids=true | all-gather | bytes 163840 | tf_op jit(solution)/shard_map/all_gather | solution.py:122
  83.3 1.3 fusion.27
  84.7 32.7 %reduce-scatter.6.cloned.1.call-done = f32[32,1024]{1,0:T(8,128)} async-done(((f32[256,1024]{1,0:T(8,128)}), f32[32,1024]{1,0:T(8,128)}) %reduce-scatter.6.cloned.1.call-update) | async-done | bytes 131088 | tf_op jit(solution)/shard_map/reduce_scatter | solution.py:124
  118.4 9.9 %all-reduce.1 = (f32[32]{0:T(128)S(1)}, f32[32]{0:T(128)S(1)}) all-reduce(f32[32]{0:T(128)S(1)} %get-tuple-element.8, f32[32]{0:T(128)S(1)} %get-tuple-element.7), channel_id=1, replica_groups=mesh['kv'=4,'tp'=8] {'kv'}, use_global_device_ids=true, to_apply=%region_7.8 | all-reduce | flops 64 | bytes 512 | tf_op jit(solution)/shard_map/psum | solution.py:24
  129.3 14.9 %all_gather.11 = bf16[256,1024]{1,0:T(8,128)(2,1)S(1)} all-gather(bf16[32,1024]{1,0:T(8,128)(2,1)S(1)} %multiply_convert_fusion.3), channel_id=1, replica_groups=mesh['kv'=4,'tp'=8] {'tp'}, dimensions={0}, use_global_device_ids=true | all-gather | bytes 589824 | tf_op jit(solution)/shard_map/all_gather | solution.py:131
  144.2 4.8 %fusion.28 = f32[256,2048]{1,0:T(8,128)} fusion(bf16[256,1024]{1,0:T(8,128)(2,1)S(1)} %all_gather.11, bf16[1024,2048]{1,0:T(8,128)(2,1)} %param.29), kind=kOutput, calls=%fused_computation.65 | convolution fusion | flops 1073741824 | bytes 6815744 | tf_op jit(solution)/shard_map/dot_general | solution.py:132
  149.0 66.0 %all-reduce.4.cloned.1.call-done = f32[256,2048]{1,0:T(8,128)} async-done(((f32[256,2048]{1,0:T(8,128)}), f32[256,2048]{1,0:T(8,128)}) %all-reduce.4.cloned.1.call-update) | async-done | bytes 2097168 | tf_op jit(solution)/shard_map/psum | solution.py:132
  215.1 5.1 %fusion = f32[256,1024]{1,0:T(8,128)} fusion(bf16[2048,1024]{1,0:T(8,128)(2,1)} %param.30, f32[256,2048]{1,0:T(8,128)} %all-reduce.4.cloned.1.call-done), kind=kOutput, calls=%fused_computation.2 | convolution fusion | flops 1075314688 | bytes 7340032 | tf_op jit(solution)/shard_map/dot_general | solution.py:136
  220.1 32.7 %reduce-scatter.8.cloned.1.call-done = f32[32,1024]{1,0:T(8,128)} async-done(((f32[256,1024]{1,0:T(8,128)}), f32[32,1024]{1,0:T(8,128)}) %reduce-scatter.8.cloned.1.call-update) | async-done | bytes 131088 | tf_op jit(solution)/shard_map/reduce_scatter | solution.py:135
  253.9 9.8 %all-reduce = (f32[32]{0:T(128)S(1)}, f32[32]{0:T(128)S(1)}) all-reduce(f32[32]{0:T(128)S(1)} %get-tuple-element.6, f32[32]{0:T(128)S(1)} %get-tuple-element.5), channel_id=1, replica_groups=mesh['kv'=4,'tp'=8] {'kv'}, use_global_device_ids=true, to_apply=%region_13.14 | all-reduce | flops 64 | bytes 512 | tf_op jit(solution)/shard_map/psum | solution.py:24
  263.8 1.6 multiply_convert_fusion.2
  (59 shorter events, 6.3 us)
Async XLA Ops:
  6.5 76.7 %copy-start = (bf16[256,1024]{1,0:T(8,128)(2,1)S(1)}, bf16[256,1024]{1,0:T(8,128)(2,1)}, u32[]{:S(2)}) copy-start(bf16[256,1024]{1,0:T(8,128)(2,1)} %param.27) | copy-start | bytes 1572868
  6.5 21.0 %copy-start.3 = (bf16[1024,256]{1,0:T(8,128)(2,1)S(1)}, bf16[1024,256]{1,0:T(8,128)(2,1)}, u32[]{:S(2)}) copy-start(bf16[1024,256]{1,0:T(8,128)(2,1)} %param.24) | copy-start | bytes 1572868
  6.5 52.0 %reduce-scatter.10.cloned.1.call-start = ((), (), s32[]{:S(2)}) async-start(), calls=%async_computation.6 | async-start | bytes 1310720
  29.3 6.5 %copy-start.8 = (f32[4]{0:T(128)S(1)}, f32[4]{0:T(128)}, u32[]{:S(2)}) copy-start(f32[4]{0:T(128)} %param.25) | copy-start | bytes 52
  29.4 88.0 %reduce-scatter.6.cloned.1.call-start = ((), (), s32[]{:S(2)}) async-start(), calls=%async_computation.3 | async-start | bytes 1179648 | tf_op jit(solution)/shard_map/reduce_scatter | solution.py:124
  42.2 8.2 %copy-start.6 = (f32[256]{0:T(256)S(1)}, f32[256]{0:T(256)}, u32[]{:S(2)}) copy-start(f32[256]{0:T(256)} %param.26) | copy-start | bytes 3076
  42.2 8.3 %copy-start.7 = (s32[64]{0:T(128)S(1)}, s32[64]{0:T(128)}, u32[]{:S(2)}) copy-start(s32[64]{0:T(128)} %param.17) | copy-start | bytes 772
  60.0 3.7 %copy-start.1 = (bf16[64,128,256]{1,2,0:T(8,128)(2,1)S(1)}, bf16[64,128,256]{1,2,0:T(8,128)(2,1)}, u32[]{:S(2)}) copy-start(bf16[64,128,256]{1,2,0:T(8,128)(2,1)} %copy.20) | copy-start | bytes 12582916
  74.3 43.0 %copy-start.2 = (bf16[32,1024]{1,0:T(8,128)(2,1)S(1)}, bf16[32,1024]{1,0:T(8,128)(2,1)}, u32[]{:S(2)}) copy-start(bf16[32,1024]{1,0:T(8,128)(2,1)} %param.16) | copy-start | bytes 196612
  74.4 53.9 %copy-start.4 = (f32[1024]{0:T(1024)S(1)}, f32[1024]{0:T(1024)}, u32[]{:S(2)}) copy-start(f32[1024]{0:T(1024)} %param.28) | copy-start | bytes 12292
  84.6 130.5 %all-reduce.4.cloned.1.call-start = ((), (), s32[]{:S(2)}) async-start(), calls=%async_computation.4 | async-start | bytes 4194304 | tf_op jit(solution)/shard_map/psum | solution.py:132
  149.0 114.8 %copy-start.5 = (f32[1024]{0:T(1024)S(1)}, f32[1024]{0:T(1024)}, u32[]{:S(2)}) copy-start(f32[1024]{0:T(1024)} %param.31) | copy-start | bytes 12292
  149.0 103.9 %reduce-scatter.8.cloned.1.call-start = ((), (), s32[]{:S(2)}) async-start(), calls=%async_computation.5 | async-start | bytes 1179648 | tf_op jit(solution)/shard_map/reduce_scatter | solution.py:135
Sparse Core Ops, SparseCore 0:
  29.5 29.0 reduce-scatter.9
  84.7 32.5 reduce-scatter.5
  149.1 65.9 all-reduce.3
  220.3 32.5 reduce-scatter.7
where the time goes:
time: 273 us; the launch traced here: 272 us
  waiting for transfers between devices  139 us (51%)
  blocking collectives  60 us (22%)
  local copies, waits for them, and re-layouts  25.8 us (9%)
  matrix products  21.4 us (8%)
  between operations  13.4 us (5%)
  other arithmetic  12 us (4%)
    psum x1, waiting for transfers between devices, per_device(): lax.psum(jnp.dot(hidden_all, up_weight, preferred_element_type=jnp.float3...  66 us
    reduce_scatter x1, waiting for transfers between devices, per_device(): lax.psum_scatter(jnp.dot(piece, down_weight, preferred_element_type=jnp.f...  32.7 us
    reduce_scatter x1, waiting for transfers between devices, per_device(): lax.psum_scatter(jnp.dot(piece, out_weight, preferred_element_type=jnp.fl...  32.7 us
    psum x2, blocking collectives, normalize(): lax.psum((jnp.sum(values, 1), jnp.sum(values * values, 1)), 'kv')  19.7 us
    unnamed x23, local copies, waits for them, and re-layouts  17.2 us
    all_gather x1, blocking collectives, per_device(): all_rows = lax.all_gather(tokens, 'tp', axis=0, tiled=True)  16.8 us
    all_gather x1, blocking collectives, per_device(): hidden_all = lax.all_gather(hidden, 'tp', axis=0, tiled=True)  14.9 us
    all_gather x1, blocking collectives, per_device(): mixed_all = lax.all_gather(mixed, 'kv', axis=0, tiled=True)  8.47 us
  transfers between devices with their start and end apart: 4, of which 4 were waited for; matrix products, arithmetic and copies ran while one was open for 8% of the time, Pallas kernels for 0%

commit v1 on v0

--- a/solution.py
+++ b/solution.py
@@ -129,7 +129,10 @@
     )
     hidden = normalize(ALPHA * tokens.astype(jnp.float32) + branch, mixer_gain).astype(jnp.bfloat16)
     hidden_all = lax.all_gather(hidden, "tp", axis=0, tiled=True)
-    upward = lax.psum(jnp.dot(hidden_all, up_weight, preferred_element_type=jnp.float32), "kv")
+    upward = jnp.sum(
+        lax.all_gather(jnp.dot(hidden_all, up_weight, preferred_element_type=jnp.float32), "kv"),
+        axis=0,
+    )
     active = jnp.square(jax.nn.relu(upward)).astype(jnp.bfloat16)
     piece = active
     downward = lax.psum_scatter(

time: 273 us -> 295 us (1.081)
  waiting for transfers between devices: 139 us -> 157 us
  other arithmetic: 12 us -> 16.4 us
    all_gather x0 -> x1, waiting for transfers between devices: none -> 84 us  [per_device(): lax.all_gather(jnp.dot(hidden_all, up_weight, preferred_element_type=jnp....]
    psum x1 -> x0, waiting for transfers between devices: 66 us -> none  [per_device(): lax.psum(jnp.dot(hidden_all, up_weight, preferred_element_type=jnp.float3...]
    reduce_sum x0 -> x1, other arithmetic: none -> 4.4 us  [per_device(): jnp.sum(lax.all_gather(jnp.dot(hidden_all, up_weight, preferred_element_t...]
  transfers between devices with their start and end apart: 4 -> 4, of which waited for: 4 -> 4; matrix products, arithmetic and copies ran while one was open for 8% -> 7% of each run, Pallas kernels for 0% -> 0%
where the time goes in v1:
time: 295 us; the launch traced here: 294 us
  waiting for transfers between devices  157 us (53%)
  blocking collectives  60 us (20%)
  local copies, waits for them, and re-layouts  25.8 us (9%)
  matrix products  20.9 us (7%)
  other arithmetic  16.4 us (6%)
  between operations  13.4 us (5%)
    all_gather x1, waiting for transfers between devices, per_device(): lax.all_gather(jnp.dot(hidden_all, up_weight, preferred_element_type=jnp....  84 us
    reduce_scatter x1, waiting for transfers between devices, per_device(): lax.psum_scatter(jnp.dot(piece, down_weight, preferred_element_type=jnp.f...  32.7 us
    reduce_scatter x1, waiting for transfers between devices, per_device(): lax.psum_scatter(jnp.dot(piece, out_weight, preferred_element_type=jnp.fl...  32.7 us
    psum x2, blocking collectives, normalize(): lax.psum((jnp.sum(values, 1), jnp.sum(values * values, 1)), 'kv')  19.7 us
    unnamed x23, local copies, waits for them, and re-layouts  17.2 us
    all_gather x1, blocking collectives, per_device(): all_rows = lax.all_gather(tokens, 'tp', axis=0, tiled=True)  16.8 us
    all_gather x1, blocking collectives, per_device(): hidden_all = lax.all_gather(hidden, 'tp', axis=0, tiled=True)  14.9 us
    all_gather x1, blocking collectives, per_device(): mixed_all = lax.all_gather(mixed, 'kv', axis=0, tiled=True)  8.47 us
  transfers between devices with their start and end apart: 4, of which 4 were waited for; matrix products, arithmetic and copies ran while one was open for 7% of the time, Pallas kernels for 0%

profile of v1, /device:TPU:0, one launch (start us, length us, event | category | flops | bytes accessed | tf_op | source)
XLA Modules:
  0.0 293.8 jit_solution(13961974019020142883)
XLA Ops:
  6.5 16.8 %all_gather.15 = bf16[256,1024]{1,0:T(8,128)(2,1)S(1)} all-gather(bf16[32,1024]{1,0:T(8,128)(2,1)} %param.16), channel_id=1, replica_groups=mesh['kv'=4,'tp'=8] {'tp'}, dimensions={0}, use_global_device_ids=true | all-gather | bytes 589824 | tf_op jit(solution)/shard_map/all_gather | solution.py:92
  23.4 1.4 fusion.22
  24.8 1.4 fusion.23
  26.2 1.4 fusion.24
  28.0 1.3 copy.37
  29.4 6.4 %copy.19 = bf16[64,128,256]{1,2,0:T(8,128)(2,1)} copy(bf16[64,128,256]{2,1,0:T(8,128)(2,1)} %param.19) | data formatting | bytes 8388608 | tf_op args[3]
  35.8 6.4 %copy.20 = bf16[64,128,256]{1,2,0:T(8,128)(2,1)} copy(bf16[64,128,256]{2,1,0:T(8,128)(2,1)} %param.20) | data formatting | bytes 8388608 | tf_op args[4]
  42.2 8.2 %reshape.187 = f32[64,64,4,64]{3,2,1,0:T(4,128)} reshape(f32[64,64,256]{2,1,0:T(8,128)} %param.18) | data formatting | bytes 8388608 | tf_op jit(solution)/shard_map/reshape | solution.py:60
  50.8 7.7 %reduce-scatter.10.cloned.1.call-done = f32[64,1024]{1,0:T(8,128)} async-done(((f32[256,1024]{1,0:T(8,128)}), f32[64,1024]{1,0:T(8,128)}) %reduce-scatter.10.cloned.1.call-update) | async-done | bytes 262160
  60.0 3.5 %fusion.26 = f32[64,4,1,128]{3,2,1,0:T(1,128)S(1)} fusion(bf16[64,4,64,1]{2,3,1,0:T(2,128)(2,1)S(1)} %copy.22, bf16[64,128,4,64]{1,3,2,0:T(8,128)(2,1)} %bitcast.43), kind=kOutput, calls=%fused_computation.63 | convolution fusion | flops 4194304 | bytes 4358144 | tf_op jit(solution)/shard_map/shn,sihn->shi/dot_general | solution.py:43
  63.7 2.3 fusion.9
  66.1 1.9 copy.39
  68.0 6.4 %multiply_reduce_fusion = f32[64,4,64]{2,1,0:T(4,128)S(1)} fusion(f32[64,64,4,64]{3,2,1,0:T(4,128)} %reshape.187, f32[64,4,64]{1,2,0:T(8,128)S(1)} %copy.39), kind=kLoop, calls=%fused_computation | loop fusion | flops 2080768 | bytes 4325376
  74.8 8.5 %all_gather.16 = bf16[256,256]{1,0:T(8,128)(2,1)S(1)} all-gather(bf16[64,256]{1,0:T(8,128)(2,1)S(1)} %copy.36), channel_id=1, replica_groups=mesh['kv'=4,'tp'=8] {'kv'}, dimensions={0}, use_global_device_ids=true | all-gather | bytes 163840 | tf_op jit(solution)/shard_map/all_gather | solution.py:122
  84.6 32.7 %reduce-scatter.6.cloned.1.call-done = f32[32,1024]{1,0:T(8,128)} async-done(((f32[256,1024]{1,0:T(8,128)}), f32[32,1024]{1,0:T(8,128)}) %reduce-scatter.6.cloned.1.call-update) | async-done | bytes 131088 | tf_op jit(solution)/shard_map/reduce_scatter | solution.py:124
  118.4 9.9 %all-reduce.1 = (f32[32]{0:T(128)S(1)}, f32[32]{0:T(128)S(1)}) all-reduce(f32[32]{0:T(128)S(1)} %get-tuple-element.8, f32[32]{0:T(128)S(1)} %get-tuple-element.7), channel_id=1, replica_groups=mesh['kv'=4,'tp'=8] {'kv'}, use_global_device_ids=true, to_apply=%region_7.8 | all-reduce | flops 64 | bytes 512 | tf_op jit(solution)/shard_map/psum | solution.py:24
  129.3 14.9 %all_gather.17 = bf16[256,1024]{1,0:T(8,128)(2,1)S(1)} all-gather(bf16[32,1024]{1,0:T(8,128)(2,1)S(1)} %multiply_convert_fusion.3), channel_id=1, replica_groups=mesh['kv'=4,'tp'=8] {'tp'}, dimensions={0}, use_global_device_ids=true | all-gather | bytes 589824 | tf_op jit(solution)/shard_map/all_gather | solution.py:131
  144.2 4.9 %fusion.28 = f32[256,2048]{1,0:T(8,128)} fusion(bf16[256,1024]{1,0:T(8,128)(2,1)S(1)} %all_gather.17, bf16[1024,2048]{1,0:T(8,128)(2,1)} %param.29), kind=kOutput, calls=%fused_computation.65 | convolution fusion | flops 1073741824 | bytes 6815744 | tf_op jit(solution)/shard_map/dot_general | solution.py:133
  149.1 84.0 %all-gather.3.cloned.1.call-done = f32[1024,2048]{1,0:T(8,128)} async-done(((f32[256,2048]{1,0:T(8,128)}), f32[1024,2048]{1,0:T(8,128)}) %all-gather.3.cloned.1.call-update) | async-done | bytes 8388624 | tf_op jit(solution)/shard_map/all_gather | solution.py:133
  233.1 4.4 %reduce_sum.67 = f32[256,2048]{1,0:T(8,128)S(1)} reduce(f32[4,256,2048]{2,1,0:T(8,128)} %bitcast.41, f32[]{:T(128)} %constant.41.clone.1), dimensions={0}, to_apply=%region_8.9 | reduce | flops 1572864 | bytes 10485764 | tf_op jit(solution)/shard_map/reduce_sum | solution.py:132
  237.6 4.4 %fusion = f32[256,1024]{1,0:T(8,128)} fusion(bf16[2048,1024]{1,0:T(8,128)(2,1)} %param.30, f32[256,2048]{1,0:T(8,128)S(1)} %reduce_sum.67), kind=kOutput, calls=%fused_computation.2 | convolution fusion | flops 1075314688 | bytes 7340032 | tf_op jit(solution)/shard_map/dot_general | solution.py:139
  242.0 32.7 %reduce-scatter.8.cloned.1.call-done = f32[32,1024]{1,0:T(8,128)} async-done(((f32[256,1024]{1,0:T(8,128)}), f32[32,1024]{1,0:T(8,128)}) %reduce-scatter.8.cloned.1.call-update) | async-done | bytes 131088 | tf_op jit(solution)/shard_map/reduce_scatter | solution.py:138
  275.8 9.8 %all-reduce = (f32[32]{0:T(128)S(1)}, f32[32]{0:T(128)S(1)}) all-reduce(f32[32]{0:T(128)S(1)} %get-tuple-element.6, f32[32]{0:T(128)S(1)} %get-tuple-element.5), channel_id=1, replica_groups=mesh['kv'=4,'tp'=8] {'kv'}, use_global_device_ids=true, to_apply=%region_13.14 | all-reduce | flops 64 | bytes 512 | tf_op jit(solution)/shard_map/psum | solution.py:24
  285.7 1.6 multiply_convert_fusion.2
  (60 shorter events, 7.6 us)
Async XLA Ops:
  6.5 76.7 %copy-start = (bf16[256,1024]{1,0:T(8,128)(2,1)S(1)}, bf16[256,1024]{1,0:T(8,128)(2,1)}, u32[]{:S(2)}) copy-start(bf16[256,1024]{1,0:T(8,128)(2,1)} %param.27) | copy-start | bytes 1572868
  6.5 21.0 %copy-start.3 = (bf16[1024,256]{1,0:T(8,128)(2,1)S(1)}, bf16[1024,256]{1,0:T(8,128)(2,1)}, u32[]{:S(2)}) copy-start(bf16[1024,256]{1,0:T(8,128)(2,1)} %param.24) | copy-start | bytes 1572868
  6.5 52.0 %reduce-scatter.10.cloned.1.call-start = ((), (), s32[]{:S(2)}) async-start(), calls=%async_computation.6 | async-start | bytes 1310720
  29.3 6.5 %copy-start.8 = (f32[4]{0:T(128)S(1)}, f32[4]{0:T(128)}, u32[]{:S(2)}) copy-start(f32[4]{0:T(128)} %param.25) | copy-start | bytes 52
  29.4 88.0 %reduce-scatter.6.cloned.1.call-start = ((), (), s32[]{:S(2)}) async-start(), calls=%async_computation.3 | async-start | bytes 1179648 | tf_op jit(solution)/shard_map/reduce_scatter | solution.py:124
  42.2 8.2 %copy-start.6 = (f32[256]{0:T(256)S(1)}, f32[256]{0:T(256)}, u32[]{:S(2)}) copy-start(f32[256]{0:T(256)} %param.26) | copy-start | bytes 3076
  42.2 8.3 %copy-start.7 = (s32[64]{0:T(128)S(1)}, s32[64]{0:T(128)}, u32[]{:S(2)}) copy-start(s32[64]{0:T(128)} %param.17) | copy-start | bytes 772
  60.0 3.7 %copy-start.1 = (bf16[64,128,256]{1,2,0:T(8,128)(2,1)S(1)}, bf16[64,128,256]{1,2,0:T(8,128)(2,1)}, u32[]{:S(2)}) copy-start(bf16[64,128,256]{1,2,0:T(8,128)(2,1)} %copy.20) | copy-start | bytes 12582916
  74.3 43.0 %copy-start.2 = (bf16[32,1024]{1,0:T(8,128)(2,1)S(1)}, bf16[32,1024]{1,0:T(8,128)(2,1)}, u32[]{:S(2)}) copy-start(bf16[32,1024]{1,0:T(8,128)(2,1)} %param.16) | copy-start | bytes 196612
  74.4 53.9 %copy-start.4 = (f32[1024]{0:T(1024)S(1)}, f32[1024]{0:T(1024)}, u32[]{:S(2)}) copy-start(f32[1024]{0:T(1024)} %param.28) | copy-start | bytes 12292
  84.6 148.5 %all-gather.3.cloned.1.call-start = ((), (), s32[]{:S(2)}) async-start(), calls=%async_computation.5 | async-start | bytes 10485760 | tf_op jit(solution)/shard_map/all_gather | solution.py:133
  149.1 125.7 %reduce-scatter.8.cloned.1.call-start = ((), (), s32[]{:S(2)}) async-start(), calls=%async_computation.4 | async-start | bytes 1179648 | tf_op jit(solution)/shard_map/reduce_scatter | solution.py:138
  237.5 48.1 %copy-start.5 = (f32[1024]{0:T(1024)S(1)}, f32[1024]{0:T(1024)}, u32[]{:S(2)}) copy-start(f32[1024]{0:T(1024)} %param.31) | copy-start | bytes 12292
Sparse Core Ops, SparseCore 0:
  29.5 29.0 reduce-scatter.9
  84.7 32.5 reduce-scatter.5
  149.2 83.8 all-gather.2
  242.1 32.5 reduce-scatter.7
